TPU v7x, 256 devices: a 4x2x16 block of a 4x16x16 slice. The times are simulated.
256 devices in a mesh: grp: 2 (over y), sp: 32 (over z, core), tp: 4 (over x).
Axes of the slice: x: 4, y: 2, z: 16, core: 2. Of those that a mesh axis runs over, the one named last changes fastest.
The devices are a block of a 4x16x16 slice.
Arguments:
- residual_in: bfloat16 [32768, 2048], P(('grp', 'sp', 'tp')), parts along dimension 0, may hold values from -6 to 6
- out_gate: bfloat16 [32768, 1024], P(('grp', 'sp', 'tp')), parts along dimension 0, may hold values from -6 to 6
- in_gate: bfloat16 [32768, 1024], P(('grp', 'sp', 'tp')), parts along dimension 0, may hold values from -6 to 6
- conv_input: bfloat16 [32768, 1024], P(('grp', 'sp', 'tp')), parts along dimension 0, may hold values from -6 to 6
- conv_kernel: bfloat16 [3, 1024], replicated, may hold values from -3.5 to 3.5
- mix_out: bfloat16 [1024, 2048], replicated, may hold values from -0.1875 to 0.1875
- post_mix_gain: float32 [2048], replicated, may hold values from 0.1 to 1.9
- pre_expert_gain: float32 [2048], replicated, may hold values from 0.1 to 1.9
- post_expert_gain: float32 [2048], replicated, may hold values from 0.1 to 1.9
- expert_ids: int32 [32768, 2], P(('grp', 'sp', 'tp')), parts along dimension 0, may hold values from 0 to 31, all different within a row; in each aligned block of 128 rows (0 to 127, 128 to 255, ...) at most 9 rows name the same one
- expert_weights: float32 [32768, 2], P(('grp', 'sp', 'tp')), parts along dimension 0, may hold values from 0.1 to 1
- gate_proj: bfloat16 [32, 2048, 2048], P('sp', None, 'tp'), may hold values from -0.375 to 0.375
- up_proj: bfloat16 [32, 2048, 2048], P('sp', None, 'tp'), may hold values from -0.375 to 0.375
- down_proj: bfloat16 [32, 2048, 2048], P('sp', 'tp'), may hold values from -0.125 to 0.125
Outputs:
- layer_out: bfloat16 [32768, 2048], P(('grp', 'sp', 'tp')), parts along dimension 0
There are 2 independent parts, one for each index of `grp`. A program takes and returns all parts, laid end to end along the dimension named above; an argument that names none is the same for every part. Nothing has to cross between parts.
Inputs may be any that keep to these rules, and one draw needn't show every extreme that they name: `expert_ids`: each row names 2 different experts. Among the 128 rows of one device no expert is named by more than 9 rows, a bound that some block reaches of them.
All inputs are finite; a program needn't handle non-finite values.
Results may differ from a plain program's by a relative error of at most 0.0095.
Values may be sent and summed in bfloat16 or wider, within the bound.
A program may use at most 64 MiB of HBM per device.

v0:
```python
import jax
import jax.numpy as jnp
from jax import lax
from jax.sharding import Mesh
from jax.sharding import PartitionSpec as P

SP_TP = ("sp_0", "sp_1", "tp")
SP = ("sp_0", "sp_1")
GRP_SP_TP = ("grp", "sp_0", "sp_1", "tp")


def from_behind(value, axis, steps):
    count = lax.axis_size(axis)
    initial, last = (max(0, -steps), min(count, count - steps))
    return lax.ppermute(value, axis, [(source, source + steps) for source in range(initial, last)])


def cut_along(array, dim, count):
    before, after = (array.shape[:dim], array.shape[dim + 1 :])
    return jnp.moveaxis(array.reshape(*before, count, -1, *after), dim, 0)


def laid_out(blocks, dim):
    dims = list(blocks.shape[1:])
    dims[dim] *= blocks.shape[0]
    return jnp.moveaxis(blocks, 0, dim).reshape(dims)


def moved_by_axis(blocks, axes, order):
    dims = [lax.axis_size(a) for a in axes]
    blocks = blocks.reshape(*dims, *blocks.shape[1:])
    for k in order:
        blocks = lax.all_to_all(blocks, axes[k], split_axis=k, concat_axis=k, tiled=True)
    return blocks.reshape(-1, *blocks.shape[len(axes) :])


def exchange_by_chip(array, groups, order, split_dim, concat_dim):
    count = lax.axis_size(groups[0]) * lax.axis_size(groups[1])
    blocks = cut_along(array, split_dim, count)
    return laid_out(moved_by_axis(blocks, groups, order), concat_dim)


def on_gathered_pieces(array, axis, dim, work, out_dim):
    rows = array.shape[dim]
    pieces = jnp.split(array, 2, axis=dim) if rows % 2 == 0 else [array]
    initial = jnp.arange(lax.axis_size(axis)) * rows
    blocks = [lax.all_gather(section, axis) for section in pieces]
    made = [jax.vmap(work)(b, initial + k * (rows // len(pieces))) for k, b in enumerate(blocks)]
    return laid_out(jnp.concatenate(made, axis=out_dim + 1), out_dim)


def summed_on_arrival(array, axis, dim):
    blocks = cut_along(array, dim, lax.axis_size(axis))
    arrived = lax.all_to_all(blocks, axis, split_axis=0, concat_axis=0, tiled=True)
    return arrived.astype(jnp.float32).sum(axis=0)


def scaled_norm(values, gain):
    return values * lax.rsqrt(jnp.mean(values * values, axis=-1, keepdims=True) + 1e-06) * gain


def slot_of(routes, experts):
    flat = routes.reshape(-1)
    onehot = (flat[:, None] == jnp.arange(experts, dtype=jnp.int32)[None, :]).astype(jnp.int32)
    before = jnp.cumsum(onehot, axis=0) - onehot
    return jnp.sum(before * onehot, axis=1)


def body(
    residual_in,
    out_gate,
    in_gate,
    conv_input,
    conv_kernel,
    mix_out,
    post_mix_gain,
    pre_expert_gain,
    post_expert_gain,
    expert_ids,
    expert_weights,
    gate_proj,
    up_proj,
    down_proj,
):
    width = mix_out.shape[1]
    inputs = in_gate.astype(jnp.float32) * conv_input.astype(jnp.float32)
    prior = from_behind(inputs[-2:], SP_TP, 1)
    padded = jnp.concatenate([prior, inputs], axis=0)
    taps = conv_kernel.astype(jnp.float32)
    conv = taps[0] * padded[:-2] + taps[1] * padded[1:-1] + taps[2] * padded[2:]
    mixed = (out_gate.astype(jnp.float32) * conv).astype(jnp.bfloat16)
    proj = jnp.dot(mixed, mix_out, preferred_element_type=jnp.float32)
    stream = (residual_in.astype(jnp.float32) + scaled_norm(proj, post_mix_gain)).astype(
        jnp.bfloat16
    )
    normed = scaled_norm(stream.astype(jnp.float32), pre_expert_gain).astype(jnp.bfloat16)
    experts = lax.axis_size(SP)
    tok_rows = normed.shape[0]
    top = expert_ids.shape[1]
    mean_rows = tok_rows * top // experts
    capacity = max(2, mean_rows + max(1, tok_rows * top // (16 * experts)))
    flat = expert_ids.reshape(-1)
    slots = slot_of(expert_ids, experts)
    owner = jnp.arange(tok_rows * top, dtype=jnp.int32) // top
    table = jnp.full((experts, capacity), tok_rows, jnp.int32).at[flat, slots].set(owner)
    padded_rows = jnp.concatenate([normed, jnp.zeros((1, width), jnp.bfloat16)], axis=0)
    outbox = padded_rows[table]
    gate_w = gate_proj[0]
    up_w = up_proj[0]
    down_w = down_proj[0]

    def expert_rows(piece):
        shape = piece.shape
        rows = piece.reshape(-1, shape[-1])
        gate = jnp.dot(rows, gate_w, preferred_element_type=jnp.float32)
        upper = jnp.dot(rows, up_w, preferred_element_type=jnp.float32)
        gate = jnp.minimum(gate, 7.0)
        upper = jnp.clip(upper, -7.0, 7.0)
        act = (gate * jax.nn.sigmoid(1.702 * gate) * (upper + 1.0)).astype(jnp.bfloat16)
        partial_value = jnp.dot(act, down_w, preferred_element_type=jnp.float32)
        return partial_value.reshape(shape[:-1] + (width,))

    def expert_piece(piece, start):
        return expert_rows(piece)

    arrived = exchange_by_chip(outbox, ("sp_0", "sp_1"), (1, 0), 0, 0)
    partial_value = on_gathered_pieces(arrived[:, None], "tp", 1, expert_piece, 1)
    summed = summed_on_arrival(partial_value.astype(jnp.bfloat16), "tp", 1).astype(jnp.bfloat16)
    returned = exchange_by_chip(summed, ("sp_0", "sp_1"), (1, 0), 0, 0).reshape(
        experts * capacity, width
    )
    picked = returned[flat * capacity + slots].astype(jnp.float32).reshape(tok_rows, top, width)
    moe = jnp.sum(picked * expert_weights[:, :, None], axis=1)
    return (stream.astype(jnp.float32) + scaled_norm(moe, post_expert_gain)).astype(jnp.bfloat16)


def solution(mesh):
    split = Mesh(
        mesh.devices.reshape(mesh.shape["grp"], 16, 2, mesh.shape["tp"]),
        ("grp", "sp_0", "sp_1", "tp"),
    )
    in_specs = (
        P(GRP_SP_TP, None),
        P(GRP_SP_TP, None),
        P(GRP_SP_TP, None),
        P(GRP_SP_TP, None),
        P(),
        P(),
        P(),
        P(),
        P(),
        P(GRP_SP_TP, None),
        P(GRP_SP_TP, None),
        P(SP, None, "tp"),
        P(SP, None, "tp"),
        P(SP, "tp", None),
    )
    out_specs = P(GRP_SP_TP, None)
    return jax.shard_map(body, mesh=split, in_specs=in_specs, out_specs=out_specs, check_vma=False)
```

profile of v0, /device:TPU:40, one launch (start us, length us, event | category | flops | bytes accessed | tf_op | source)
XLA Modules:
  0.0 365.7 jit_solution(7495995657394759271)
XLA Ops:
  6.6 1.2 convert_multiply_fusion.2
  7.8 3.6 collective-permute-start
  11.4 0.8 copy.46
  12.2 0.1 eq.29
  12.3 0.1 eq.25
  12.5 0.1 reshape.134
  12.6 0.8 fusion.34
  13.4 0.6 reduce-window.6
  14.0 0.2 slice_reduce_fusion
  14.3 0.1 fusion.30
  14.4 12.8 %scatter_fusion = s32[32,9]{0,1:T(8,128)S(1)} fusion(s32[32,9]{0,1:T(8,128)S(1)} %broadcast_in_dim.4, s32[256]{0:T(256)S(1)} %bitcast.57, s32[256]{0:T(256)S(1)} %and_select_fusion), kind=kCustom, calls=%fused_computation.2 | custom fusion | bytes 5120 | tf_op jit(solution)/shard_map/scatter | solution.py:105
  27.2 0.1 copy.50
  27.3 0.1 reshape.141
  27.5 3.2 multiply_reduce_fusion.2
  30.6 0.4 fusion.12
  31.0 0.8 copy-done.1
  31.8 0.2 fusion.14
  32.1 3.0 gather_fusion
  35.0 2.7 reshape_reshape.6
  37.7 2.3 copy.51
  40.0 4.7 %all_to_all.25 = bf16[16,2,1,9,2048]{4,0,3,2,1:T(8,128)(2,1)S(1)} all-to-all(bf16[16,2,1,9,2048]{4,0,3,2,1:T(8,128)(2,1)S(1)} %copy.51), channel_id=1, replica_groups=mesh['grp'=2,'sp_0'=16,'sp_1'=2,'tp'=4] {'sp_1'}, dimensions={1} | all-to-all | bytes 2359296 | tf_op jit(solution)/shard_map/all_to_all | solution.py:33
  44.7 1.2 copy.52
  45.9 82.9 %all_to_all.26 = bf16[16,2,1,9,2048]{4,1,3,2,0:T(2,128)(2,1)S(1)} all-to-all(bf16[16,2,1,9,2048]{4,1,3,2,0:T(2,128)(2,1)S(1)} %copy.52), channel_id=1, replica_groups=mesh['grp'=2,'sp_0'=16,'sp_1'=2,'tp'=4] {'sp_0'}, dimensions={0} | all-to-all | bytes 2359296 | tf_op jit(solution)/shard_map/all_to_all | solution.py:33
  128.8 0.9 copy.53
  129.8 1.5 all_gather_broadcast_in_dim_reshape_reshape.3
  131.2 0.1 all-gather.2.cloned.1.call-update
  131.3 52.4 %all-gather.2.cloned.1.call-done = bf16[4,32,1,9,2048]{4,1,3,2,0:T(8,128)(2,1)} async-done(((bf16[1,32,1,9,2048]{4,1,3,2,0:T(8,128)(2,1)}), bf16[4,32,1,9,2048]{4,1,3,2,0:T(8,128)(2,1)}) %all-gather.2.cloned.1.call-update) | async-done | bytes 4718608 | tf_op jit(solution)/shard_map/all_gather | solution.py:47
  183.7 6.1 %copy.54 = bf16[4,32,1,9,2048]{4,0,3,1,2:T(4,128)(2,1)S(1)} copy(bf16[4,32,1,9,2048]{4,1,3,2,0:T(8,128)(2,1)} %all-gather.2.cloned.1.call-done) | data formatting | bytes 9437184 | tf_op jit(solution)/shard_map/all_gather | solution.py:47
  189.8 5.4 %fusion = f32[4,288,512]{2,1,0:T(8,128)S(1)} fusion(bf16[4,288,2048]{2,0,1:T(4,128)(2,1)S(1)} %bitcast.58, bf16[1,2048,512]{2,1,0:T(8,128)(2,1)S(1)} %copy-done.8), kind=kOutput, calls=%fused_computation.5 | convolution fusion | flops 2415919104 | bytes 9175040 | tf_op jit(solution)/shard_map/vmap()/dot_general | solution.py:116
  195.2 6.4 %multiply_convert_fusion = bf16[4,288,512]{2,1,0:T(8,128)(2,1)S(1)} fusion(f32[4,288,512]{2,1,0:T(8,128)S(1)} %fusion, bf16[1,2048,512]{2,1,0:T(8,128)(2,1)S(1)} %copy-done.9, bf16[4,288,2048]{2,0,1:T(4,128)(2,1)S(1)} %bitcast.59), kind=kOutput, calls=%fused_computation.9 | convolution fusion | flops 2421817344 | bytes 10354688 | tf_op jit(solution)/shard_map/vmap()/dot_general | solution.py:115
  201.6 0.9 copy.57
  202.5 2.8 convert_bitcast_fusion
  205.4 57.5 %all_to_all.27 = bf16[4,32,1,9,2048]{4,1,3,2,0:T(8,128)(2,1)S(1)} all-to-all(bf16[4,32,1,9,2048]{4,1,3,2,0:T(8,128)(2,1)S(1)} %convert_bitcast_fusion), channel_id=1, replica_groups=mesh['grp'=2,'sp_0'=16,'sp_1'=2,'tp'=4] {'tp'}, dimensions={0} | all-to-all | bytes 9437184 | tf_op jit(solution)/shard_map/all_to_all | solution.py:54
  262.9 2.0 bitcast_reduce_fusion
  264.9 2.9 reshape_reshape.7
  267.7 0.4 copy.61
  268.2 4.7 %all_to_all.28 = bf16[16,2,1,1,9,2048]{5,0,4,3,2,1:T(8,128)(2,1)S(1)} all-to-all(bf16[16,2,1,1,9,2048]{5,0,4,3,2,1:T(8,128)(2,1)S(1)} %copy.61), channel_id=1, replica_groups=mesh['grp'=2,'sp_0'=16,'sp_1'=2,'tp'=4] {'sp_1'}, dimensions={1} | all-to-all | bytes 2359296 | tf_op jit(solution)/shard_map/all_to_all | solution.py:33
  272.9 2.2 copy.62
  275.1 12.7 %all-to-all-start.4 = ((bf16[16,2,1,1,9,2048]{5,1,4,3,2,0:T(2,128)(2,1)}), bf16[16,2,1,1,9,2048]{5,1,4,3,2,0:T(2,128)(2,1)S(1)}, u32[]{:S(2)}, u32[]{:S(2)}) async-start(bf16[16,2,1,1,9,2048]{5,1,4,3,2,0:T(2,128)(2,1)} %copy.62), calls=%async_computation.4 | async-start | bytes 2359296 | tf_op jit(solution)/shard_map/all_to_all | solution.py:33
  287.8 0.1 copy.64
  287.9 54.9 %all-to-all-done.4 = bf16[16,2,1,1,9,2048]{5,1,4,3,2,0:T(2,128)(2,1)S(1)} async-done(((bf16[16,2,1,1,9,2048]{5,1,4,3,2,0:T(2,128)(2,1)}), bf16[16,2,1,1,9,2048]{5,1,4,3,2,0:T(2,128)(2,1)S(1)}, u32[]{:S(2)}, u32[]{:S(2)}) %all-to-all-start.4) | async-done | bytes 1179680 | tf_op jit(solution)/shard_map/all_to_all | solution.py:33
  342.8 2.0 copy.63
  344.8 1.8 reshape_reshape_reshape.3
  346.6 2.3 gather_fusion.1
  349.0 3.4 reshape.138
  352.4 4.9 %multiply_reduce_fusion = f32[128,2048]{1,0:T(8,128)S(1)} fusion(f32[128,2,2048]{2,1,0:T(2,128)} %reshape.138, f32[128,2]{1,0:T(8,128)S(1)} %copy.64), kind=kLoop, calls=%fused_computation.13 | loop fusion | flops 786432 | bytes 3146752 | tf_op jit(solution)/shard_map/reduce_sum | solution.py:133
  357.2 0.2 multiply_reduce_fusion.1
  357.4 1.0 fusion.15
  (37 shorter events, 0.2 us)
Async XLA Ops:
  6.5 196.0 %copy-start = (bf16[1,512,2048]{2,1,0:T(8,128)(2,1)S(1)}, bf16[1,512,2048]{2,1,0:T(8,128)(2,1)}, u32[]{:S(2)}) copy-start(bf16[1,512,2048]{2,1,0:T(8,128)(2,1)} %param.27) | copy-start | bytes 6291460
  6.6 20.9 %copy-start.10 = (bf16[128,1024]{1,0:T(8,128)(2,1)S(1)}, bf16[128,1024]{1,0:T(8,128)(2,1)}, u32[]{:S(2)}) copy-start(bf16[128,1024]{1,0:T(8,128)(2,1)} %param.15) | copy-start | bytes 786436
  6.6 177.1 %all-gather.2.cloned.1.call-start = ((), (), s32[]{:S(2)}) async-start(), calls=%async_computation.5 | async-start | bytes 5898240 | tf_op jit(solution)/shard_map/all_gather | solution.py:47
  7.8 19.6 %collective-permute-start = (f32[2,1024]{1,0:T(2,128)S(1)}, f32[2,1024]{1,0:T(2,128)S(1)}, u32[]{:S(2)}, u32[]{:S(2)}) collective-permute-start(f32[2,1024]{1,0:T(2,128)S(1)} %slice.39), channel_id=1, source_target_pairs={{0,1},{1,2},{2,3},{3,4},{4,5},{5,6},{6,7},{7,8},{8,9},{9,10},{10,1... | collective-permute-start | bytes 24584 | tf_op jit(solution)/shard_map/ppermute | solution.py:15
  27.4 3.2 copy-start.3
  27.4 3.2 copy-start.4
  30.6 1.2 copy-start.5
  31.0 0.8 copy-start.1
  183.7 6.1 %copy-start.8 = (bf16[1,2048,512]{2,1,0:T(8,128)(2,1)S(1)}, bf16[1,2048,512]{2,1,0:T(8,128)(2,1)}, u32[]{:S(2)}) copy-start(bf16[1,2048,512]{2,1,0:T(8,128)(2,1)} %param.26) | copy-start | bytes 6291460
  189.8 5.4 %copy-start.9 = (bf16[1,2048,512]{2,1,0:T(8,128)(2,1)S(1)}, bf16[1,2048,512]{2,1,0:T(8,128)(2,1)}, u32[]{:S(2)}) copy-start(bf16[1,2048,512]{2,1,0:T(8,128)(2,1)} %param.25) | copy-start | bytes 6291460
  272.9 14.9 %copy-start.7 = (f32[128,2]{0,1:T(2,128)S(1)}, f32[128,2]{0,1:T(2,128)}, u32[]{:S(2)}) copy-start(f32[128,2]{0,1:T(2,128)} %param.24) | copy-start | bytes 3076
  275.1 67.7 %all-to-all-start.4 = ((bf16[16,2,1,1,9,2048]{5,1,4,3,2,0:T(2,128)(2,1)}), bf16[16,2,1,1,9,2048]{5,1,4,3,2,0:T(2,128)(2,1)S(1)}, u32[]{:S(2)}, u32[]{:S(2)}) async-start(bf16[16,2,1,1,9,2048]{5,1,4,3,2,0:T(2,128)(2,1)} %copy.62), calls=%async_computation.4 | async-start | bytes 2359296 | tf_op jit(solution)/shard_map/all_to_all | solution.py:33
  352.4 5.0 %copy-start.2 = (bf16[128,2048]{1,0:T(8,128)(2,1)S(1)}, bf16[128,2048]{1,0:T(8,128)(2,1)}, u32[]{:S(2)}) copy-start(bf16[128,2048]{1,0:T(8,128)(2,1)} %copy-done.1) | copy-start | bytes 1572868
  352.4 5.0 %copy-start.6 = (f32[2048]{0:T(1024)S(1)}, f32[2048]{0:T(1024)}, u32[]{:S(2)}) copy-start(f32[2048]{0:T(1024)} %param.22) | copy-start | bytes 24580
Sparse Core Ops, SparseCore 0:
  131.4 52.2 all-gather.1
where the time goes:
time: 372 us; the launch traced here: 366 us
  blocking collectives  150 us (40%)
  waiting for transfers between devices  107 us (29%)
  local copies, waits for them, and re-layouts  49.8 us (13%)
  matrix products  17.7 us (5%)
  starting transfers between devices  16.2 us (4%)
  between operations  14.2 us (4%)
  other arithmetic  10.7 us (3%)
    all_to_all x3, blocking collectives, moved_by_axis(): lax.all_to_all(blocks, axes[k], split_axis=k, concat_axis=k, tiled=True)  92.3 us
    all_to_all x1, blocking collectives, summed_on_arrival(): lax.all_to_all(blocks, axis, split_axis=0, concat_axis=0, tiled=True)  57.5 us
    all_to_all x1, waiting for transfers between devices, moved_by_axis(): lax.all_to_all(blocks, axes[k], split_axis=k, concat_axis=k, tiled=True)  54.9 us
    all_gather x1, waiting for transfers between devices, on_gathered_pieces(): blocks = [lax.all_gather(section, axis) for section in pieces]  52.4 us
    scatter x1, local copies, waits for them, and re-layouts, body(): jnp.full((experts, capacity), tok_rows, jnp.int32).at[flat, slots]  12.8 us
    all_to_all x1, starting transfers between devices, moved_by_axis(): lax.all_to_all(blocks, axes[k], split_axis=k, concat_axis=k, tiled=True)  12.7 us
    another operation x4, local copies, waits for them, and re-layouts, moved_by_axis(): blocks = blocks.reshape(*dims, *blocks.shape[1:])  8.25 us
  transfers between devices with their start and end apart: 3, of which 2 were waited for; matrix products, arithmetic and copies ran while one was open for 4% of the time, Pallas kernels for 0%

commit v1 on v0

v1 whole, which is shorter than its diff:
```python
import functools

import jax
import jax.numpy as jnp
from jax import lax
from jax.experimental import pallas as pl
from jax.experimental.pallas import tpu as pltpu
from jax.sharding import PartitionSpec as P

TOKENS_OVER = ("grp", "sp", "tp")
MESH = pl.DeviceIdType.MESH
F32 = jnp.float32
BF16 = jnp.bfloat16
LANES = 128
ROWS = 8
EPS = 1e-06


def dot(a, b):
    return jnp.dot(a, b, preferred_element_type=F32)


def layer_kernel(
    n_sp,
    n_tp,
    ids_ref,
    wts_ref,
    taps_ref,
    post_mix_ref,
    pre_exp_ref,
    post_exp_ref,
    in_gate_hbm,
    conv_in_hbm,
    out_gate_hbm,
    resid_hbm,
    mix_hbm,
    gate_hbm,
    up_hbm,
    down_hbm,
    out_ref,
    in_gate,
    conv_in,
    out_gate,
    resid,
    mix_w,
    gate_w,
    up_w,
    down_w,
    halo_g,
    halo_c,
    mixed,
    wide,
    stream,
    normed,
    pick,
    outbox,
    rows_in,
    parts_out,
    relay_a,
    relay_b,
    from_left,
    from_right,
    summed,
    returned,
    tail,
    x_rows,
    act,
    r_rows,
    r_last,
    load_sem,
    halo_send,
    halo_recv,
    z_send,
    z_recv,
    g_send,
    g_recv,
    f_send,
    f_recv,
    p_send,
    p_recv,
    d_send,
    d_recv,
    s_send,
    s_recv,
    b_send,
    b_recv,
):
    tokens, width = resid.shape
    conv_w = in_gate.shape[1]
    hidden = gate_w.shape[1]
    chunks = width // LANES
    n_z = n_sp // 2
    steps = n_z // 2
    n_main = n_sp * ROWS
    n_rows = n_main + n_sp
    me = lax.axis_index("sp")
    z, core = me // 2, me % 2
    x = lax.axis_index("tp")
    right = (x + 1) % n_tp
    left = (x + n_tp - 1) % n_tp
    place = me * n_tp + x
    after = (place + 1) % (n_sp * n_tp)
    before = (place + n_sp * n_tp - 1) % (n_sp * n_tp)

    def device_at(p):
        return {"sp": p // n_tp, "tp": p % n_tp}

    bar = pltpu.get_barrier_semaphore()

    def greet(d, carry):
        pl.semaphore_signal(bar, inc=1, device_id={"sp": (me + d) % n_sp}, device_id_type=MESH)
        return carry

    lax.fori_loop(1, n_sp, greet, 0)
    for who in ({"tp": right}, {"tp": left}, device_at(after), device_at(before)):
        pl.semaphore_signal(bar, inc=1, device_id=who, device_id_type=MESH)

    loads = [
        pltpu.make_async_copy(src, dst, load_sem.at[k])
        for k, (src, dst) in enumerate(
            (
                (in_gate_hbm, in_gate),
                (conv_in_hbm, conv_in),
                (out_gate_hbm, out_gate),
                (mix_hbm, mix_w),
                (resid_hbm, resid),
                (gate_hbm, gate_w),
                (up_hbm, up_w),
                (down_hbm, down_w),
            )
        )
    ]
    for load in loads:
        load.start()

    ids = ids_ref[...]
    e_z, e_core = ids // 2, ids % 2
    dz = (e_z - z + n_z) % n_z
    far = dz >= steps
    step_of = jnp.where(far, dz - steps, (steps - dz) % steps)
    message = step_of * 4 + jnp.where(far, 2, 0) + (e_core + core) % 2
    place_iota = lax.broadcasted_iota(jnp.int32, (n_sp, tokens), 0)
    hot = [(place_iota == message[k : k + 1, :]) for k in range(2)]
    both = hot[0].astype(F32) + hot[1].astype(F32)
    earlier = (
        lax.broadcasted_iota(jnp.int32, (tokens, tokens), 0)
        < lax.broadcasted_iota(jnp.int32, (tokens, tokens), 1)
    ).astype(F32)
    count = dot(both.astype(BF16), earlier.astype(BF16))
    row_iota = lax.broadcasted_iota(jnp.int32, (n_rows, tokens), 0)
    gather = []
    for k in range(2):
        slot = jnp.sum(jnp.where(hot[k], count, 0.0), axis=0, keepdims=True).astype(jnp.int32)
        msg = message[k : k + 1, :]
        code = jnp.where(slot < ROWS, msg * ROWS + slot, n_main + msg)
        gather.append((row_iota == code).astype(F32))
    spread = (gather[0] + gather[1]).astype(BF16)

    pl.semaphore_wait(bar, n_sp - 1 + 4)

    halo_rows = halo_g.shape[0]
    halos = []
    for k, (src, dst) in enumerate(((in_gate, halo_g), (conv_in, halo_c))):
        halos.append(
            pltpu.make_async_remote_copy(
                src_ref=src.at[pl.ds(tokens - halo_rows, halo_rows)],
                dst_ref=dst,
                send_sem=halo_send.at[k],
                recv_sem=halo_recv.at[k],
                device_id=device_at(after),
                device_id_type=MESH,
            )
        )
        loads[k].wait()
        halos[k].start()
    loads[2].wait()
    for halo in halos:
        halo.wait_recv()

    taps = taps_ref[...].astype(F32)
    starts = (place == 0).astype(F32)
    col = 256
    for c in range(0, conv_w, col):
        cols = slice(c, c + col)
        u = in_gate[:, cols].astype(F32) * conv_in[:, cols].astype(F32)
        head = halo_g[:, cols].astype(F32) * halo_c[:, cols].astype(F32) * (1.0 - starts)
        padded = jnp.concatenate([head, u], axis=0)
        one = pltpu.roll(padded, 1, 0)[halo_rows:]
        two = pltpu.roll(padded, 2, 0)[halo_rows:]
        conv = taps[0:1, cols] * two + taps[1:2, cols] * one + taps[2:3, cols] * u
        mixed[:, cols] = (out_gate[:, cols].astype(F32) * conv).astype(BF16)
    for halo in halos:
        halo.wait_send()

    loads[3].wait()
    loads[4].wait()
    tile = 512
    square = jnp.zeros((tokens, LANES), F32)

    def fold(v):
        total = v[:, :LANES]
        for k in range(LANES, v.shape[1], LANES):
            total = total + v[:, k : k + LANES]
        return total

    for c in range(0, width, tile):
        cols = slice(c, c + tile)
        proj = dot(mixed[...], mix_w[:, cols])
        wide[:, cols] = proj
        square = square + fold(proj * proj)
    scale = lax.rsqrt(jnp.sum(square, axis=1, keepdims=True) * (1.0 / width) + EPS)
    square = jnp.zeros((tokens, LANES), F32)
    for c in range(0, width, tile):
        cols = slice(c, c + tile)
        s = resid[:, cols].astype(F32) + wide[:, cols] * scale * post_mix_ref[:, cols]
        s = s.astype(BF16)
        stream[:, cols] = s
        s = s.astype(F32)
        square = square + fold(s * s)
    scale = lax.rsqrt(jnp.sum(square, axis=1, keepdims=True) * (1.0 / width) + EPS)
    for c in range(0, width, tile):
        cols = slice(c, c + tile)
        normed[:, cols] = (stream[:, cols].astype(F32) * scale * pre_exp_ref[:, cols]).astype(BF16)

    def pack_main(store, rows, c, count_of):
        pair = [
            rows[: count_of * ROWS, k * LANES : (k + 1) * LANES].reshape(count_of, ROWS, LANES)
            for k in range(2)
        ]
        store(c, jnp.concatenate(pair, axis=1).astype(BF16))

    for c in range(0, chunks, 2):
        rows = dot(spread, normed[:, c * LANES : (c + 2) * LANES])

        def store(c, block):
            outbox[:, c * ROWS : (c + 2) * ROWS, :] = block

        pack_main(store, rows, c, n_sp)
        for k in range(2):
            tail[pl.ds(c + k, n_sp, stride=chunks), :] = rows[
                n_main:, k * LANES : (k + 1) * LANES
            ]
    outbox[:, chunks * ROWS :, :] = tail[...].reshape(n_sp, chunks, LANES).astype(BF16)

    def expert_at(m):
        step, half, cc = m // 4, (m // 2) % 2, m % 2
        far_z = (1 - half) * ((steps - step) % steps) + half * (steps + step)
        return {"sp": ((z + far_z) % n_z) * 2 + (core + cc) % 2}

    def source_at(m):
        step, half, cc = m // 4, (m // 2) % 2, m % 2
        far_z = (1 - half) * ((steps - step) % steps) + half * (steps + step)
        return {"sp": ((z + n_z - far_z) % n_z) * 2 + (core + cc) % 2}

    def dispatch(m):
        return pltpu.make_async_remote_copy(
            src_ref=outbox.at[m],
            dst_ref=rows_in.at[0, m],
            send_sem=z_send.at[m],
            recv_sem=z_recv.at[m],
            device_id=expert_at(m),
            device_id_type=MESH,
        )

    def give_back(m):
        return pltpu.make_async_remote_copy(
            src_ref=summed.at[m],
            dst_ref=returned.at[m],
            send_sem=b_send.at[m],
            recv_sem=b_recv.at[m],
            device_id=source_at(m),
            device_id_type=MESH,
        )

    own_in = pltpu.make_async_copy(outbox.at[0], rows_in.at[0, 0], z_recv.at[0])
    own_back = pltpu.make_async_copy(summed.at[0], returned.at[0], b_recv.at[0])

    def send_out(m, carry):
        dispatch(m).start()
        return carry

    lax.fori_loop(1, n_sp, send_out, 0)
    own_in.start()

    def side(to, src, dst, send, recv):
        return pltpu.make_async_remote_copy(
            src_ref=src,
            dst_ref=dst,
            send_sem=send,
            recv_sem=recv,
            device_id={"tp": to},
            device_id_type=MESH,
        )

    def spread_x(t):
        four = pl.ds(4 * t, 4)
        return (
            side(right, rows_in.at[0, four], rows_in.at[1, four], g_send.at[0, t], g_recv.at[0, t]),
            side(left, rows_in.at[0, four], rows_in.at[3, four], g_send.at[1, t], g_recv.at[1, t]),
        )

    def forward_x(t):
        a, b = pl.ds(4 * t, 2), pl.ds(4 * t + 2, 2)
        return (
            side(right, rows_in.at[1, a], rows_in.at[2, a], f_send.at[0, t], f_recv.at[0, t]),
            side(left, rows_in.at[3, b], rows_in.at[2, b], f_send.at[1, t], f_recv.at[1, t]),
        )

    def across(t):
        a, b = pl.ds(4 * t, 2), pl.ds(4 * t + 2, 2)
        return (
            side(right, parts_out.at[2, a], relay_a.at[t], p_send.at[0, t], p_recv.at[0, t]),
            side(left, parts_out.at[2, b], relay_b.at[t], p_send.at[1, t], p_recv.at[1, t]),
        )

    def direct(t):
        a, b = pl.ds(4 * t, 2), pl.ds(4 * t + 2, 2)
        return (
            side(right, parts_out.at[3, b], from_left.at[b], d_send.at[0, t], d_recv.at[0, t]),
            side(left, parts_out.at[1, a], from_right.at[a], d_send.at[1, t], d_recv.at[1, t]),
        )

    def relayed(t):
        a, b = pl.ds(4 * t, 2), pl.ds(4 * t + 2, 2)
        return (
            side(right, parts_out.at[3, a], from_left.at[a], s_send.at[0, t], s_recv.at[0, t]),
            side(left, parts_out.at[1, b], from_right.at[b], s_send.at[1, t], s_recv.at[1, t]),
        )

    for k in range(2):
        padded = jnp.concatenate(
            [gather[k], jnp.zeros((-n_rows % LANES, tokens), F32)], axis=0
        )
        pick[k * tokens : (k + 1) * tokens, :] = padded.T.astype(BF16)[:, :n_rows]

    def arrive(t):
        def landed(j, carry):
            dispatch(4 * t + j).wait_recv()
            return carry

        lax.fori_loop(0, 4, landed, 0)
        for c in spread_x(t):
            c.start()

    def forward(t):
        for c in spread_x(t):
            c.wait_recv()
        for c in forward_x(t):
            c.start()

    m_in = 4 * n_tp
    main_in = m_in * ROWS

    def experts(t):
        for c in forward_x(t):
            c.wait_recv()
        four = pl.ds(4 * t, 4)
        for q in range(n_tp):
            tail[q * 4 * chunks : (q + 1) * 4 * chunks, :] = (
                rows_in[q, four, chunks * ROWS :, :].astype(F32).reshape(4 * chunks, LANES)
            )
        for c in range(0, chunks, 2):
            block = rows_in[:, four, c * ROWS : (c + 2) * ROWS, :].astype(F32)
            block = block.reshape(m_in, 2 * ROWS, LANES)
            for k in range(2):
                main = block[:, k * ROWS : (k + 1) * ROWS, :].reshape(main_in, LANES)
                last = tail[pl.ds(c + k, m_in, stride=chunks), :]
                x_rows[:, (c + k) * LANES : (c + k + 1) * LANES] = jnp.concatenate(
                    [main, last], axis=0
                ).astype(BF16)
        half = 256
        for c in range(0, hidden, half):
            cols = slice(c, c + half)
            gate = dot(x_rows[...], gate_w[:, cols])
            up = dot(x_rows[...], up_w[:, cols])
            gate = jnp.minimum(gate, 7.0)
            up = jnp.clip(up, -7.0, 7.0)
            act[:, cols] = (gate * jax.nn.sigmoid(1.702 * gate) * (up + 1.0)).astype(BF16)
        for c in range(0, chunks, 2):
            rows = dot(act[...], down_w[:, c * LANES : (c + 2) * LANES])

            def store(c, block):
                parts_out[:, four, c * ROWS : (c + 2) * ROWS, :] = block.reshape(
                    n_tp, 4, 2 * ROWS, LANES
                )

            pack_main(store, rows, c, m_in)
            for k in range(2):
                tail[pl.ds(c + k, m_in, stride=chunks), :] = rows[
                    main_in:, k * LANES : (k + 1) * LANES
                ]
        for q in range(n_tp):
            parts_out[q, four, chunks * ROWS :, :] = (
                tail[q * 4 * chunks : (q + 1) * 4 * chunks, :]
                .reshape(4, chunks, LANES)
                .astype(BF16)
            )
        for c in across(t):
            c.start()
        for c in direct(t):
            c.start()

    def add_relay(t):
        a, b = pl.ds(4 * t, 2), pl.ds(4 * t + 2, 2)
        for c in across(t):
            c.wait_recv()
        parts_out[3, a] = (parts_out[3, a].astype(F32) + relay_a[t].astype(F32)).astype(BF16)
        parts_out[1, b] = (parts_out[1, b].astype(F32) + relay_b[t].astype(F32)).astype(BF16)
        for c in relayed(t):
            c.start()

    def finish(t):
        four = pl.ds(4 * t, 4)
        for c in direct(t):
            c.wait_recv()
        for c in relayed(t):
            c.wait_recv()
        total = from_left[four].astype(F32) + from_right[four].astype(F32)
        summed[four] = (total + parts_out[0, four].astype(F32)).astype(BF16)

        def back(j, carry):
            give_back(4 * t + j).start()
            return carry

        @pl.when(t == 0)
        def _():
            own_back.start()

        lax.fori_loop((t == 0).astype(jnp.int32), 4, back, 0)

    stages = (finish, add_relay, experts, forward, arrive)

    def pipeline(s, carry):
        for k, stage in enumerate(stages):
            t = s - (len(stages) - 1 - k)
            if stage is experts:

                @pl.when(t == 0)
                def _():
                    for load in loads[5:]:
                        load.wait()

            @pl.when((t >= 0) & (t < steps))
            def _():
                stage(t)

        return carry

    lax.fori_loop(0, steps + len(stages) - 1, pipeline, 0)

    for t in range(steps):
        for j in range(4):
            give_back(4 * t + j).wait_recv()
        four = slice(4 * t, 4 * t + 4)
        tail[: 4 * chunks, :] = (
            returned[four, chunks * ROWS :, :].astype(F32).reshape(4 * chunks, LANES)
        )
        for c in range(0, chunks, 2):
            block = returned[four, c * ROWS : (c + 2) * ROWS, :].astype(F32)
            for k in range(2):
                main = block[:, k * ROWS : (k + 1) * ROWS, :].reshape(4 * ROWS, LANES)
                cols = slice((c + k) * LANES, (c + k + 1) * LANES)
                r_rows[4 * t * ROWS : 4 * (t + 1) * ROWS, cols] = main.astype(BF16)
                r_last[4 * t : 4 * t + 4, cols] = tail[pl.ds(c + k, 4, stride=chunks), :]
    weights = jnp.concatenate([wts_ref[...], jnp.zeros((LANES - 2, tokens), F32)], axis=0).T
    square = jnp.zeros((tokens, LANES), F32)
    for c in range(0, width, tile):
        cols = slice(c, c + tile)
        two = dot(pick[:, :n_main], r_rows[:, cols]) + dot(
            pick[:, n_main:], r_last[:, cols].astype(BF16)
        )
        moe = two[:tokens] * weights[:, 0:1] + two[tokens:] * weights[:, 1:2]
        wide[:, cols] = moe
        square = square + fold(moe * moe)
    scale = lax.rsqrt(jnp.sum(square, axis=1, keepdims=True) * (1.0 / width) + EPS)
    for c in range(0, width, tile):
        cols = slice(c, c + tile)
        out_ref[:, cols] = (
            stream[:, cols].astype(F32) + wide[:, cols] * scale * post_exp_ref[:, cols]
        ).astype(BF16)

    def drain(m, carry):
        dispatch(m).wait_send()
        give_back(m).wait_send()
        return carry

    lax.fori_loop(1, n_sp, drain, 0)

    def drain_x(t, carry):
        for copies in (spread_x(t), forward_x(t), across(t), direct(t), relayed(t)):
            for c in copies:
                c.wait_send()
        return carry

    lax.fori_loop(0, steps, drain_x, 0)


def layer(
    n_sp,
    n_tp,
    residual_in,
    out_gate,
    in_gate,
    conv_input,
    conv_kernel,
    mix_out,
    post_mix_gain,
    pre_expert_gain,
    post_expert_gain,
    expert_ids,
    expert_weights,
    gate_proj,
    up_proj,
    down_proj,
):
    tokens, width = residual_in.shape
    conv_w = in_gate.shape[1]
    hidden = gate_proj.shape[2]
    chunks = width // LANES
    steps = n_sp // 4
    msg = (ROWS + 1) * chunks
    n_main = n_sp * ROWS
    rows_step = 4 * n_tp * (ROWS + 1)
    vmem = pl.BlockSpec(memory_space=pltpu.VMEM)
    anyspace = pl.BlockSpec(memory_space=pl.ANY)
    dma = pltpu.SemaphoreType.DMA
    scratch = [
        pltpu.VMEM((tokens, conv_w), BF16),
        pltpu.VMEM((tokens, conv_w), BF16),
        pltpu.VMEM((tokens, conv_w), BF16),
        pltpu.VMEM((tokens, width), BF16),
        pltpu.VMEM((conv_w, width), BF16),
        pltpu.VMEM((width, hidden), BF16),
        pltpu.VMEM((width, hidden), BF16),
        pltpu.VMEM((hidden, width), BF16),
        pltpu.VMEM((16, conv_w), BF16),
        pltpu.VMEM((16, conv_w), BF16),
        pltpu.VMEM((tokens, conv_w), BF16),
        pltpu.VMEM((tokens, width), F32),
        pltpu.VMEM((tokens, width), BF16),
        pltpu.VMEM((tokens, width), BF16),
        pltpu.VMEM((2 * tokens, n_main + n_sp), BF16),
        pltpu.VMEM((n_sp, msg, LANES), BF16),
        pltpu.VMEM((n_tp, n_sp, msg, LANES), BF16),
        pltpu.VMEM((n_tp, n_sp, msg, LANES), BF16),
        pltpu.VMEM((steps, 2, msg, LANES), BF16),
        pltpu.VMEM((steps, 2, msg, LANES), BF16),
        pltpu.VMEM((n_sp, msg, LANES), BF16),
        pltpu.VMEM((n_sp, msg, LANES), BF16),
        pltpu.VMEM((n_sp, msg, LANES), BF16),
        pltpu.VMEM((n_sp, msg, LANES), BF16),
        pltpu.VMEM((n_sp * chunks, LANES), F32),
        pltpu.VMEM((rows_step, width), BF16),
        pltpu.VMEM((rows_step, hidden), BF16),
        pltpu.VMEM((n_main, width), BF16),
        pltpu.VMEM((n_sp, width), F32),
        dma((8,)),
        dma((2,)),
        dma((2,)),
        dma((n_sp,)),
        dma((n_sp,)),
    ]
    scratch += [dma((2, steps)) for _ in range(10)]
    scratch += [dma((n_sp,)), dma((n_sp,))]
    return pl.pallas_call(
        functools.partial(layer_kernel, n_sp, n_tp),
        out_shape=jax.ShapeDtypeStruct((tokens, width), BF16),
        in_specs=[vmem] * 6 + [anyspace] * 8,
        out_specs=vmem,
        scratch_shapes=scratch,
        compiler_params=pltpu.CompilerParams(
            collective_id=0, has_side_effects=True, vmem_limit_bytes=62 * 1024 * 1024
        ),
    )(
        expert_ids.T,
        expert_weights.T,
        conv_kernel,
        post_mix_gain.reshape(1, width),
        pre_expert_gain.reshape(1, width),
        post_expert_gain.reshape(1, width),
        in_gate,
        conv_input,
        out_gate,
        residual_in,
        mix_out,
        gate_proj[0],
        up_proj[0],
        down_proj[0],
    )


def solution(mesh):
    tok = P(TOKENS_OVER, None)
    in_specs = (tok, tok, tok, tok, P(), P(), P(), P(), P(), tok, tok)
    in_specs += (P("sp", None, "tp"), P("sp", None, "tp"), P("sp", "tp", None))
    return jax.shard_map(
        functools.partial(layer, mesh.shape["sp"], mesh.shape["tp"]),
        mesh=mesh,
        in_specs=in_specs,
        out_specs=tok,
        check_vma=False,
    )
```

time: 372 us -> 147 us (0.40); the launches traced: 366 us -> 146 us
  blocking collectives: 150 us -> 0 us
  Pallas kernels: 0 us -> 144 us
  waiting for transfers between devices: 107 us -> 0 us
  local copies, waits for them, and re-layouts: 49.8 us -> 1.88 us
  matrix products: 17.7 us -> 0 us
  starting transfers between devices: 16.2 us -> 0 us
  between operations: 14.2 us -> 0.01 us
  other arithmetic: 10.7 us -> 0 us
    all_to_all x4 -> x0, blocking collectives: 150 us -> none  [the longest x3 92.3 us: moved_by_axis(): lax.all_to_all(blocks, axes[k], split_axis=k, concat_axis=k, tiled=True)]
    pallas_call x0 -> x1, Pallas kernels: none -> 144 us  [layer(): pl.pallas_call(functools.partial(layer_kernel, n_sp, n_tp), out_shape=jax...]
    all_to_all x1 -> x0, waiting for transfers between devices: 54.9 us -> none  [moved_by_axis(): lax.all_to_all(blocks, axes[k], split_axis=k, concat_axis=k, tiled=True)]
    all_gather x1 -> x0, waiting for transfers between devices: 52.4 us -> none  [on_gathered_pieces(): blocks = [lax.all_gather(section, axis) for section in pieces]]
    dot_general x4 -> x0, matrix products: 17.7 us -> none  [the longest x1 6.4 us: expert_rows(): gate = jnp.dot(rows, gate_w, preferred_element_type=jnp.float32)]
    scatter x1 -> x0, local copies, waits for them, and re-layouts: 12.8 us -> none  [body(): jnp.full((experts, capacity), tok_rows, jnp.int32).at[flat, slots]]
    all_to_all x1 -> x0, starting transfers between devices: 12.7 us -> none  [moved_by_axis(): lax.all_to_all(blocks, axes[k], split_axis=k, concat_axis=k, tiled=True)]
    another operation x7 -> x0, local copies, waits for them, and re-layouts: 11.5 us -> none  [the longest x4 8.25 us: moved_by_axis(): blocks = blocks.reshape(*dims, *blocks.shape[1:])]
  transfers between devices with their start and end apart: 3 -> 0, of which waited for: 2 -> 0; matrix products, arithmetic and copies ran while one was open for 4% -> 0% of each run, Pallas kernels for 0% -> 0%
where the time goes in v1:
time: 147 us; the launch traced here: 146 us
  Pallas kernels  144 us (98%)
  local copies, waits for them, and re-layouts  1.88 us (1%)
    pallas_call x1, Pallas kernels, layer(): pl.pallas_call(functools.partial(layer_kernel, n_sp, n_tp), out_shape=jax...  144 us

profile of v1, /device:TPU:40, one launch (start us, length us, event | category | flops | bytes accessed | tf_op | source)
XLA Modules:
  0.0 145.7 jit_solution(11794220998630428743)
XLA Ops:
  0.0 143.8 %shard_map.136 = bf16[128,2048]{1,0:T(8,128)(2,1)} custom-call(s32[2,128]{1,0:T(2,128)} %bitcast.14, f32[2,128]{1,0:T(2,128)} %bitcast.15, bf16[3,1024]{1,0:T(4,128)(2,1)} %taps_ref.1, f32[1,2048]{1,0:T(1,128)} %bitcast.11, f32[1,2048]{1,0:T(1,128)} %bitcast.12, f32[1,2048]{1,0:T(1,128)} %bitcast.13, bf16[128,1024]{1,0:T(8,128)(2,1)} %in_gate_hbm.1, ...), custom_call_target="tpu_custom_call" | custom-call | tf_op jit(solution)/shard_map/pallas_call | solution.py:565
  143.8 1.9 %copy.16 = bf16[128,2048]{1,0:T(8,128)(2,1)} copy(bf16[128,2048]{1,0:T(8,128)(2,1)} %shard_map.136) | data formatting | bytes 1048576

commit v2 on v1

--- a/solution.py
+++ b/solution.py
@@ -37,7 +37,7 @@
     gate_hbm,
     up_hbm,
     down_hbm,
-    out_ref,
+    out_hbm,
     in_gate,
     conv_in,
     out_gate,
@@ -46,6 +46,8 @@
     gate_w,
     up_w,
     down_w,
+    edge_g,
+    edge_c,
     halo_g,
     halo_c,
     mixed,
@@ -56,10 +58,8 @@
     outbox,
     rows_in,
     parts_out,
-    relay_a,
-    relay_b,
-    from_left,
-    from_right,
+    relay,
+    sides,
     summed,
     returned,
     tail,
@@ -67,23 +67,17 @@
     act,
     r_rows,
     r_last,
+    out_rows,
     load_sem,
     halo_send,
     halo_recv,
-    z_send,
     z_recv,
-    g_send,
     g_recv,
-    f_send,
     f_recv,
-    p_send,
     p_recv,
-    d_send,
-    d_recv,
-    s_send,
     s_recv,
-    b_send,
     b_recv,
+    sent,
 ):
     tokens, width = resid.shape
     conv_w = in_gate.shape[1]
@@ -107,13 +101,21 @@
 
     bar = pltpu.get_barrier_semaphore()
 
-    def greet(d, carry):
-        pl.semaphore_signal(bar, inc=1, device_id={"sp": (me + d) % n_sp}, device_id_type=MESH)
+    def enter(who):
+        pl.semaphore_signal(bar, inc=1, device_id=who, device_id_type=MESH)
+
+    def greet(k, carry):
+        far_up = steps - (k + 1) // 2
+        up = far_up + (k % 2) * (n_z - 2 * far_up)
+        for c in range(2):
+            enter({"sp": ((z + up) % n_z) * 2 + c})
         return carry
 
-    lax.fori_loop(1, n_sp, greet, 0)
-    for who in ({"tp": right}, {"tp": left}, device_at(after), device_at(before)):
-        pl.semaphore_signal(bar, inc=1, device_id=who, device_id_type=MESH)
+    lax.fori_loop(0, n_z - 1, greet, 0)
+    for who in ({"sp": me + 1 - 2 * core}, device_at(after), device_at(before)):
+        enter(who)
+    for who in ({"tp": right}, {"tp": left}):
+        enter(who)
 
     loads = [
         pltpu.make_async_copy(src, dst, load_sem.at[k])
@@ -156,44 +158,43 @@
         gather.append((row_iota == code).astype(F32))
     spread = (gather[0] + gather[1]).astype(BF16)
 
+    for load, src, edge in ((loads[0], in_gate, edge_g), (loads[1], conv_in, edge_c)):
+        load.wait()
+        edge[...] = src[tokens - 2 :, :]
+
     pl.semaphore_wait(bar, n_sp - 1 + 4)
 
-    halo_rows = halo_g.shape[0]
-    halos = []
-    for k, (src, dst) in enumerate(((in_gate, halo_g), (conv_in, halo_c))):
-        halos.append(
-            pltpu.make_async_remote_copy(
-                src_ref=src.at[pl.ds(tokens - halo_rows, halo_rows)],
-                dst_ref=dst,
-                send_sem=halo_send.at[k],
-                recv_sem=halo_recv.at[k],
-                device_id=device_at(after),
-                device_id_type=MESH,
-            )
+    halos = [
+        pltpu.make_async_remote_copy(
+            src_ref=src,
+            dst_ref=dst,
+            send_sem=halo_send.at[k],
+            recv_sem=halo_recv.at[k],
+            device_id=device_at(after),
+            device_id_type=MESH,
         )
-        loads[k].wait()
-        halos[k].start()
-    loads[2].wait()
+        for k, (src, dst) in enumerate(((edge_g, halo_g), (edge_c, halo_c)))
+    ]
+    for halo in halos:
+        halo.start()
+    for load in loads[2:5]:
+        load.wait()
     for halo in halos:
         halo.wait_recv()
 
     taps = taps_ref[...].astype(F32)
-    starts = (place == 0).astype(F32)
+    row_of = lax.broadcasted_iota(jnp.int32, (tokens, 1), 0)
+    inside = (place > 0).astype(F32)
     col = 256
     for c in range(0, conv_w, col):
         cols = slice(c, c + col)
         u = in_gate[:, cols].astype(F32) * conv_in[:, cols].astype(F32)
-        head = halo_g[:, cols].astype(F32) * halo_c[:, cols].astype(F32) * (1.0 - starts)
-        padded = jnp.concatenate([head, u], axis=0)
-        one = pltpu.roll(padded, 1, 0)[halo_rows:]
-        two = pltpu.roll(padded, 2, 0)[halo_rows:]
+        head = halo_g[:, cols].astype(F32) * halo_c[:, cols].astype(F32) * inside
+        one = jnp.where(row_of == 0, head[1:2], pltpu.roll(u, 1, 0))
+        two = jnp.where(row_of == 1, head[1:2], pltpu.roll(u, 2, 0))
+        two = jnp.where(row_of == 0, head[0:1], two)
         conv = taps[0:1, cols] * two + taps[1:2, cols] * one + taps[2:3, cols] * u
         mixed[:, cols] = (out_gate[:, cols].astype(F32) * conv).astype(BF16)
-    for halo in halos:
-        halo.wait_send()
-
-    loads[3].wait()
-    loads[4].wait()
     tile = 512
     square = jnp.zeros((tokens, LANES), F32)
 
@@ -252,80 +253,53 @@
         far_z = (1 - half) * ((steps - step) % steps) + half * (steps + step)
         return {"sp": ((z + n_z - far_z) % n_z) * 2 + (core + cc) % 2}
 
+    def took(ref, sem):
+        pltpu.make_async_copy(ref, ref, sem).wait()
+
     def dispatch(m):
-        return pltpu.make_async_remote_copy(
+        pltpu.make_async_remote_copy(
             src_ref=outbox.at[m],
             dst_ref=rows_in.at[0, m],
-            send_sem=z_send.at[m],
-            recv_sem=z_recv.at[m],
+            send_sem=sent.at[0],
+            recv_sem=z_recv.at[m // 4],
             device_id=expert_at(m),
             device_id_type=MESH,
-        )
+        ).start()
 
     def give_back(m):
-        return pltpu.make_async_remote_copy(
+        pltpu.make_async_remote_copy(
             src_ref=summed.at[m],
             dst_ref=returned.at[m],
-            send_sem=b_send.at[m],
-            recv_sem=b_recv.at[m],
+            send_sem=sent.at[1],
+            recv_sem=b_recv.at[m // 4],
             device_id=source_at(m),
             device_id_type=MESH,
-        )
-
-    own_in = pltpu.make_async_copy(outbox.at[0], rows_in.at[0, 0], z_recv.at[0])
-    own_back = pltpu.make_async_copy(summed.at[0], returned.at[0], b_recv.at[0])
-
-    def send_out(m, carry):
-        dispatch(m).start()
+        ).start()
+
+    def order(t):
+        return (t + steps - 1) % steps
+
+    def send_out(k, carry):
+        m = (k + n_sp - 4) % n_sp
+
+        @pl.when(m > 0)
+        def _():
+            dispatch(m)
+
         return carry
 
-    lax.fori_loop(1, n_sp, send_out, 0)
-    own_in.start()
+    pltpu.make_async_copy(outbox.at[0], rows_in.at[0, 0], z_recv.at[0]).start()
+    lax.fori_loop(0, n_sp, send_out, 0)
 
     def side(to, src, dst, send, recv):
-        return pltpu.make_async_remote_copy(
+        pltpu.make_async_remote_copy(
             src_ref=src,
             dst_ref=dst,
-            send_sem=send,
+            send_sem=sent.at[send],
             recv_sem=recv,
             device_id={"tp": to},
             device_id_type=MESH,
-        )
-
-    def spread_x(t):
-        four = pl.ds(4 * t, 4)
-        return (
-            side(right, rows_in.at[0, four], rows_in.at[1, four], g_send.at[0, t], g_recv.at[0, t]),
-            side(left, rows_in.at[0, four], rows_in.at[3, four], g_send.at[1, t], g_recv.at[1, t]),
-        )
-
-    def forward_x(t):
-        a, b = pl.ds(4 * t, 2), pl.ds(4 * t + 2, 2)
-        return (
-            side(right, rows_in.at[1, a], rows_in.at[2, a], f_send.at[0, t], f_recv.at[0, t]),
-            side(left, rows_in.at[3, b], rows_in.at[2, b], f_send.at[1, t], f_recv.at[1, t]),
-        )
-
-    def across(t):
-        a, b = pl.ds(4 * t, 2), pl.ds(4 * t + 2, 2)
-        return (
-            side(right, parts_out.at[2, a], relay_a.at[t], p_send.at[0, t], p_recv.at[0, t]),
-            side(left, parts_out.at[2, b], relay_b.at[t], p_send.at[1, t], p_recv.at[1, t]),
-        )
-
-    def direct(t):
-        a, b = pl.ds(4 * t, 2), pl.ds(4 * t + 2, 2)
-        return (
-            side(right, parts_out.at[3, b], from_left.at[b], d_send.at[0, t], d_recv.at[0, t]),
-            side(left, parts_out.at[1, a], from_right.at[a], d_send.at[1, t], d_recv.at[1, t]),
-        )
-
-    def relayed(t):
-        a, b = pl.ds(4 * t, 2), pl.ds(4 * t + 2, 2)
-        return (
-            side(right, parts_out.at[3, a], from_left.at[a], s_send.at[0, t], s_recv.at[0, t]),
-            side(left, parts_out.at[1, b], from_right.at[b], s_send.at[1, t], s_recv.at[1, t]),
-        )
+        ).start()
 
     for k in range(2):
         padded = jnp.concatenate(
@@ -334,27 +308,23 @@
         pick[k * tokens : (k + 1) * tokens, :] = padded.T.astype(BF16)[:, :n_rows]
 
     def arrive(t):
-        def landed(j, carry):
-            dispatch(4 * t + j).wait_recv()
-            return carry
-
-        lax.fori_loop(0, 4, landed, 0)
-        for c in spread_x(t):
-            c.start()
+        four = pl.ds(4 * t, 4)
+        took(rows_in.at[0, four], z_recv.at[t])
+        side(right, rows_in.at[0, four], rows_in.at[1, four], 2, g_recv.at[t])
+        side(left, rows_in.at[0, four], rows_in.at[3, four], 2, g_recv.at[t])
 
     def forward(t):
-        for c in spread_x(t):
-            c.wait_recv()
-        for c in forward_x(t):
-            c.start()
+        a, b = pl.ds(4 * t, 2), pl.ds(4 * t + 2, 2)
+        took(rows_in.at[pl.ds(0, 2), pl.ds(4 * t, 4)], g_recv.at[t])
+        side(right, rows_in.at[1, a], rows_in.at[2, a], 3, f_recv.at[t])
+        side(left, rows_in.at[3, b], rows_in.at[2, b], 3, f_recv.at[t])
 
     m_in = 4 * n_tp
     main_in = m_in * ROWS
 
     def experts(t):
-        for c in forward_x(t):
-            c.wait_recv()
         four = pl.ds(4 * t, 4)
+        took(rows_in.at[2, four], f_recv.at[t])
         for q in range(n_tp):
             tail[q * 4 * chunks : (q + 1) * 4 * chunks, :] = (
                 rows_in[q, four, chunks * ROWS :, :].astype(F32).reshape(4 * chunks, LANES)
@@ -395,38 +365,35 @@
                 .reshape(4, chunks, LANES)
                 .astype(BF16)
             )
-        for c in across(t):
-            c.start()
-        for c in direct(t):
-            c.start()
+        a, b = pl.ds(4 * t, 2), pl.ds(4 * t + 2, 2)
+        side(right, parts_out.at[2, a], relay.at[t, pl.ds(0, 2)], 4, p_recv.at[t])
+        side(left, parts_out.at[2, b], relay.at[t, pl.ds(2, 2)], 4, p_recv.at[t])
+        side(right, parts_out.at[3, b], sides.at[0, b], 5, s_recv.at[t])
+        side(left, parts_out.at[1, a], sides.at[1, a], 5, s_recv.at[t])
 
     def add_relay(t):
         a, b = pl.ds(4 * t, 2), pl.ds(4 * t + 2, 2)
-        for c in across(t):
-            c.wait_recv()
-        parts_out[3, a] = (parts_out[3, a].astype(F32) + relay_a[t].astype(F32)).astype(BF16)
-        parts_out[1, b] = (parts_out[1, b].astype(F32) + relay_b[t].astype(F32)).astype(BF16)
-        for c in relayed(t):
-            c.start()
+        took(relay.at[t], p_recv.at[t])
+        parts_out[3, a] = (parts_out[3, a].astype(F32) + relay[t, 0:2].astype(F32)).astype(BF16)
+        parts_out[1, b] = (parts_out[1, b].astype(F32) + relay[t, 2:4].astype(F32)).astype(BF16)
+        side(right, parts_out.at[3, a], sides.at[0, a], 6, s_recv.at[t])
+        side(left, parts_out.at[1, b], sides.at[1, b], 6, s_recv.at[t])
 
     def finish(t):
         four = pl.ds(4 * t, 4)
-        for c in direct(t):
-            c.wait_recv()
-        for c in relayed(t):
-            c.wait_recv()
-        total = from_left[four].astype(F32) + from_right[four].astype(F32)
+        took(sides.at[:, four], s_recv.at[t])
+        total = sides[0, four].astype(F32) + sides[1, four].astype(F32)
         summed[four] = (total + parts_out[0, four].astype(F32)).astype(BF16)
 
         def back(j, carry):
-            give_back(4 * t + j).start()
+            give_back(4 * t + j)
             return carry
+
+        lax.fori_loop((t == 0).astype(jnp.int32), 4, back, 0)
 
         @pl.when(t == 0)
         def _():
-            own_back.start()
-
-        lax.fori_loop((t == 0).astype(jnp.int32), 4, back, 0)
+            pltpu.make_async_copy(summed.at[0], returned.at[0], b_recv.at[0]).start()
 
     stages = (finish, add_relay, experts, forward, arrive)
 
@@ -442,16 +409,16 @@
 
             @pl.when((t >= 0) & (t < steps))
             def _():
-                stage(t)
+                stage(order(t))
 
         return carry
 
     lax.fori_loop(0, steps + len(stages) - 1, pipeline, 0)
 
-    for t in range(steps):
-        for j in range(4):
-            give_back(4 * t + j).wait_recv()
+    for k in range(steps):
+        t = order(k)
         four = slice(4 * t, 4 * t + 4)
+        took(returned.at[pl.ds(4 * t, 4)], b_recv.at[t])
         tail[: 4 * chunks, :] = (
             returned[four, chunks * ROWS :, :].astype(F32).reshape(4 * chunks, LANES)
         )
@@ -462,6 +429,11 @@
                 cols = slice((c + k) * LANES, (c + k + 1) * LANES)
                 r_rows[4 * t * ROWS : 4 * (t + 1) * ROWS, cols] = main.astype(BF16)
                 r_last[4 * t : 4 * t + 4, cols] = tail[pl.ds(c + k, 4, stride=chunks), :]
+
+    def out_copy(c):
+        cols = pl.ds(c, tile)
+        return pltpu.make_async_copy(out_rows.at[:, cols], out_hbm.at[:, cols], sent.at[7])
+
     weights = jnp.concatenate([wts_ref[...], jnp.zeros((LANES - 2, tokens), F32)], axis=0).T
     square = jnp.zeros((tokens, LANES), F32)
     for c in range(0, width, tile):
@@ -475,24 +447,20 @@
     scale = lax.rsqrt(jnp.sum(square, axis=1, keepdims=True) * (1.0 / width) + EPS)
     for c in range(0, width, tile):
         cols = slice(c, c + tile)
-        out_ref[:, cols] = (
+        out_rows[:, cols] = (
             stream[:, cols].astype(F32) + wide[:, cols] * scale * post_exp_ref[:, cols]
         ).astype(BF16)
-
-    def drain(m, carry):
-        dispatch(m).wait_send()
-        give_back(m).wait_send()
-        return carry
-
-    lax.fori_loop(1, n_sp, drain, 0)
-
-    def drain_x(t, carry):
-        for copies in (spread_x(t), forward_x(t), across(t), direct(t), relayed(t)):
-            for c in copies:
-                c.wait_send()
-        return carry
-
-    lax.fori_loop(0, steps, drain_x, 0)
+        out_copy(c).start()
+
+    for halo in halos:
+        halo.wait_send()
+    took(outbox.at[pl.ds(1, n_sp - 1)], sent.at[0])
+    took(summed.at[pl.ds(1, n_sp - 1)], sent.at[1])
+    took(rows_in.at[pl.ds(0, 2)], sent.at[2])
+    took(rows_in.at[0], sent.at[3])
+    for k in range(4, 7):
+        took(parts_out.at[0], sent.at[k])
+    took(out_rows, sent.at[7])
 
 
 def layer(
@@ -533,8 +501,10 @@
         pltpu.VMEM((width, hidden), BF16),
         pltpu.VMEM((width, hidden), BF16),
         pltpu.VMEM((hidden, width), BF16),
-        pltpu.VMEM((16, conv_w), BF16),
-        pltpu.VMEM((16, conv_w), BF16),
+        pltpu.VMEM((2, conv_w), BF16),
+        pltpu.VMEM((2, conv_w), BF16),
+        pltpu.VMEM((2, conv_w), BF16),
+        pltpu.VMEM((2, conv_w), BF16),
         pltpu.VMEM((tokens, conv_w), BF16),
         pltpu.VMEM((tokens, width), F32),
         pltpu.VMEM((tokens, width), BF16),
@@ -543,10 +513,8 @@
         pltpu.VMEM((n_sp, msg, LANES), BF16),
         pltpu.VMEM((n_tp, n_sp, msg, LANES), BF16),
         pltpu.VMEM((n_tp, n_sp, msg, LANES), BF16),
-        pltpu.VMEM((steps, 2, msg, LANES), BF16),
-        pltpu.VMEM((steps, 2, msg, LANES), BF16),
-        pltpu.VMEM((n_sp, msg, LANES), BF16),
-        pltpu.VMEM((n_sp, msg, LANES), BF16),
+        pltpu.VMEM((steps, 4, msg, LANES), BF16),
+        pltpu.VMEM((2, n_sp, msg, LANES), BF16),
         pltpu.VMEM((n_sp, msg, LANES), BF16),
         pltpu.VMEM((n_sp, msg, LANES), BF16),
         pltpu.VMEM((n_sp * chunks, LANES), F32),
@@ -554,19 +522,18 @@
         pltpu.VMEM((rows_step, hidden), BF16),
         pltpu.VMEM((n_main, width), BF16),
         pltpu.VMEM((n_sp, width), F32),
+        pltpu.VMEM((tokens, width), BF16),
         dma((8,)),
         dma((2,)),
         dma((2,)),
-        dma((n_sp,)),
-        dma((n_sp,)),
     ]
-    scratch += [dma((2, steps)) for _ in range(10)]
-    scratch += [dma((n_sp,)), dma((n_sp,))]
+    scratch += [dma((steps,)) for _ in range(6)]
+    scratch += [dma((8,))]
     return pl.pallas_call(
         functools.partial(layer_kernel, n_sp, n_tp),
         out_shape=jax.ShapeDtypeStruct((tokens, width), BF16),
         in_specs=[vmem] * 6 + [anyspace] * 8,
-        out_specs=vmem,
+        out_specs=anyspace,
         scratch_shapes=scratch,
         compiler_params=pltpu.CompilerParams(
             collective_id=0, has_side_effects=True, vmem_limit_bytes=62 * 1024 * 1024

time: 147 us -> 140 us (0.952)
  Pallas kernels: 144 us -> 137 us
    pallas_call x1, Pallas kernels: 144 us -> 137 us  [layer(): pl.pallas_call(functools.partial(layer_kernel, n_sp, n_tp), out_shape=jax...]
where the time goes in v2:
time: 140 us; the launch traced here: 139 us
  Pallas kernels  137 us (98%)
  local copies, waits for them, and re-layouts  1.88 us (1%)
    pallas_call x1, Pallas kernels, layer(): pl.pallas_call(functools.partial(layer_kernel, n_sp, n_tp), out_shape=jax...  137 us

profile of v2, /device:TPU:40, one launch (start us, length us, event | category | flops | bytes accessed | tf_op | source)
XLA Modules:
  0.0 139.1 jit_solution(11253401400414869135)
XLA Ops:
  0.0 137.2 %shard_map.136 = bf16[128,2048]{1,0:T(8,128)(2,1)} custom-call(s32[2,128]{1,0:T(2,128)} %bitcast.14, f32[2,128]{1,0:T(2,128)} %bitcast.15, bf16[3,1024]{1,0:T(4,128)(2,1)} %taps_ref.1, f32[1,2048]{1,0:T(1,128)} %bitcast.11, f32[1,2048]{1,0:T(1,128)} %bitcast.12, f32[1,2048]{1,0:T(1,128)} %bitcast.13, bf16[128,1024]{1,0:T(8,128)(2,1)} %in_gate_hbm.1, ...), custom_call_target="tpu_custom_call" | custom-call | tf_op jit(solution)/shard_map/pallas_call | solution.py:532
  137.2 1.9 %copy.16 = bf16[128,2048]{1,0:T(8,128)(2,1)} copy(bf16[128,2048]{1,0:T(8,128)(2,1)} %shard_map.136) | data formatting | bytes 1048576

commit v3 on v2

--- a/solution.py
+++ b/solution.py
@@ -23,12 +23,12 @@
 def layer_kernel(
     n_sp,
     n_tp,
-    ids_ref,
-    wts_ref,
-    taps_ref,
-    post_mix_ref,
-    pre_exp_ref,
-    post_exp_ref,
+    ids_hbm,
+    wts_hbm,
+    taps_hbm,
+    post_mix_hbm,
+    pre_exp_hbm,
+    post_exp_hbm,
     in_gate_hbm,
     conv_in_hbm,
     out_gate_hbm,
@@ -38,6 +38,12 @@
     up_hbm,
     down_hbm,
     out_hbm,
+    ids_ref,
+    wts_ref,
+    taps_ref,
+    post_mix_ref,
+    pre_exp_ref,
+    post_exp_ref,
     in_gate,
     conv_in,
     out_gate,
@@ -129,11 +135,18 @@
                 (gate_hbm, gate_w),
                 (up_hbm, up_w),
                 (down_hbm, down_w),
+                (ids_hbm, ids_ref),
+                (taps_hbm, taps_ref),
+                (post_mix_hbm, post_mix_ref),
+                (pre_exp_hbm, pre_exp_ref),
+                (wts_hbm, wts_ref),
+                (post_exp_hbm, post_exp_ref),
             )
         )
     ]
-    for load in loads:
+    for load in loads[:2] + loads[8:10] + loads[2:5] + loads[10:] + loads[5:8]:
         load.start()
+    loads[8].wait()
 
     ids = ids_ref[...]
     e_z, e_core = ids // 2, ids % 2
@@ -162,6 +175,28 @@
         load.wait()
         edge[...] = src[tokens - 2 :, :]
 
+    head_rows = 16
+    inside = (place > 0).astype(F32)
+    loads[9].wait()
+    taps = taps_ref[...].astype(F32)
+
+    def convolve(rows, with_halo):
+        row_of = lax.broadcasted_iota(jnp.int32, (rows, 1), 0)
+        col = 256
+        for c in range(0, conv_w, col):
+            cols = slice(c, c + col)
+            u = in_gate[:rows, cols].astype(F32) * conv_in[:rows, cols].astype(F32)
+            one, two = pltpu.roll(u, 1, 0), pltpu.roll(u, 2, 0)
+            if with_halo:
+                head = halo_g[:, cols].astype(F32) * halo_c[:, cols].astype(F32) * inside
+                one = jnp.where(row_of == 0, head[1:2], one)
+                two = jnp.where(row_of == 1, head[1:2], two)
+                two = jnp.where(row_of == 0, head[0:1], two)
+            conv = taps[0:1, cols] * two + taps[1:2, cols] * one + taps[2:3, cols] * u
+            mixed[:rows, cols] = (out_gate[:rows, cols].astype(F32) * conv).astype(BF16)
+
+    loads[2].wait()
+    convolve(tokens, False)
     pl.semaphore_wait(bar, n_sp - 1 + 4)
 
     halos = [
@@ -177,24 +212,12 @@
     ]
     for halo in halos:
         halo.start()
-    for load in loads[2:5]:
+    for load in loads[3:5] + loads[10:]:
         load.wait()
     for halo in halos:
         halo.wait_recv()
-
-    taps = taps_ref[...].astype(F32)
-    row_of = lax.broadcasted_iota(jnp.int32, (tokens, 1), 0)
-    inside = (place > 0).astype(F32)
-    col = 256
-    for c in range(0, conv_w, col):
-        cols = slice(c, c + col)
-        u = in_gate[:, cols].astype(F32) * conv_in[:, cols].astype(F32)
-        head = halo_g[:, cols].astype(F32) * halo_c[:, cols].astype(F32) * inside
-        one = jnp.where(row_of == 0, head[1:2], pltpu.roll(u, 1, 0))
-        two = jnp.where(row_of == 1, head[1:2], pltpu.roll(u, 2, 0))
-        two = jnp.where(row_of == 0, head[0:1], two)
-        conv = taps[0:1, cols] * two + taps[1:2, cols] * one + taps[2:3, cols] * u
-        mixed[:, cols] = (out_gate[:, cols].astype(F32) * conv).astype(BF16)
+    convolve(head_rows, True)
+
     tile = 512
     square = jnp.zeros((tokens, LANES), F32)
 
@@ -404,7 +427,7 @@
 
                 @pl.when(t == 0)
                 def _():
-                    for load in loads[5:]:
+                    for load in loads[5:8]:
                         load.wait()
 
             @pl.when((t >= 0) & (t < steps))
@@ -489,10 +512,15 @@
     msg = (ROWS + 1) * chunks
     n_main = n_sp * ROWS
     rows_step = 4 * n_tp * (ROWS + 1)
-    vmem = pl.BlockSpec(memory_space=pltpu.VMEM)
     anyspace = pl.BlockSpec(memory_space=pl.ANY)
     dma = pltpu.SemaphoreType.DMA
     scratch = [
+        pltpu.VMEM((2, tokens), jnp.int32),
+        pltpu.VMEM((2, tokens), F32),
+        pltpu.VMEM(conv_kernel.shape, BF16),
+        pltpu.VMEM((1, width), F32),
+        pltpu.VMEM((1, width), F32),
+        pltpu.VMEM((1, width), F32),
         pltpu.VMEM((tokens, conv_w), BF16),
         pltpu.VMEM((tokens, conv_w), BF16),
         pltpu.VMEM((tokens, conv_w), BF16),
@@ -523,7 +551,7 @@
         pltpu.VMEM((n_main, width), BF16),
         pltpu.VMEM((n_sp, width), F32),
         pltpu.VMEM((tokens, width), BF16),
-        dma((8,)),
+        dma((14,)),
         dma((2,)),
         dma((2,)),
     ]
@@ -532,7 +560,7 @@
     return pl.pallas_call(
         functools.partial(layer_kernel, n_sp, n_tp),
         out_shape=jax.ShapeDtypeStruct((tokens, width), BF16),
-        in_specs=[vmem] * 6 + [anyspace] * 8,
+        in_specs=[anyspace] * 14,
         out_specs=anyspace,
         scratch_shapes=scratch,
         compiler_params=pltpu.CompilerParams(

time: 140 us -> 139 us (level)
  no operation moved by 1% of the time
where the time goes in v3:
time: 139 us; the launch traced here: 138 us
  Pallas kernels  136 us (98%)
  local copies, waits for them, and re-layouts  1.88 us (1%)
    pallas_call x1, Pallas kernels, layer(): pl.pallas_call(functools.partial(layer_kernel, n_sp, n_tp), out_shape=jax...  136 us

profile of v3, /device:TPU:40, one launch (start us, length us, event | category | flops | bytes accessed | tf_op | source)
XLA Modules:
  0.0 138.4 jit_solution(10623989227000401761)
XLA Ops:
  0.0 136.5 %shard_map.136 = bf16[128,2048]{1,0:T(8,128)(2,1)} custom-call(s32[2,128]{1,0:T(2,128)} %bitcast.14, f32[2,128]{1,0:T(2,128)} %bitcast.15, bf16[3,1024]{1,0:T(4,128)(2,1)} %taps_hbm.1, f32[1,2048]{1,0:T(1,128)} %bitcast.11, f32[1,2048]{1,0:T(1,128)} %bitcast.12, f32[1,2048]{1,0:T(1,128)} %bitcast.13, bf16[128,1024]{1,0:T(8,128)(2,1)} %in_gate_hbm.1, ...), custom_call_target="tpu_custom_call" | custom-call | tf_op jit(solution)/shard_map/pallas_call | solution.py:560
  136.5 1.9 %copy.16 = bf16[128,2048]{1,0:T(8,128)(2,1)} copy(bf16[128,2048]{1,0:T(8,128)(2,1)} %shard_map.136) | data formatting | bytes 1048576

commit v4 on v3

--- a/solution.py
+++ b/solution.py
@@ -302,17 +302,10 @@
     def order(t):
         return (t + steps - 1) % steps
 
-    def send_out(k, carry):
-        m = (k + n_sp - 4) % n_sp
-
-        @pl.when(m > 0)
-        def _():
-            dispatch(m)
-
-        return carry
-
     pltpu.make_async_copy(outbox.at[0], rows_in.at[0, 0], z_recv.at[0]).start()
-    lax.fori_loop(0, n_sp, send_out, 0)
+    for k in range(n_sp):
+        if (k + n_sp - 4) % n_sp > 0:
+            dispatch((k + n_sp - 4) % n_sp)
 
     def side(to, src, dst, send, recv):
         pltpu.make_async_remote_copy(

time: 139 us -> 139 us (level)
  no operation moved by 1% of the time
where the time goes in v4:
time: 139 us; the launch traced here: 138 us
  Pallas kernels  136 us (98%)
  local copies, waits for them, and re-layouts  1.88 us (1%)
    pallas_call x1, Pallas kernels, layer(): pl.pallas_call(functools.partial(layer_kernel, n_sp, n_tp), out_shape=jax...  136 us

profile of v4, /device:TPU:40, one launch (start us, length us, event | category | flops | bytes accessed | tf_op | source)
XLA Modules:
  0.0 138.3 jit_solution(5774316482991509337)
XLA Ops:
  0.0 136.4 %shard_map.136 = bf16[128,2048]{1,0:T(8,128)(2,1)} custom-call(s32[2,128]{1,0:T(2,128)} %bitcast.14, f32[2,128]{1,0:T(2,128)} %bitcast.15, bf16[3,1024]{1,0:T(4,128)(2,1)} %taps_hbm.1, f32[1,2048]{1,0:T(1,128)} %bitcast.11, f32[1,2048]{1,0:T(1,128)} %bitcast.12, f32[1,2048]{1,0:T(1,128)} %bitcast.13, bf16[128,1024]{1,0:T(8,128)(2,1)} %in_gate_hbm.1, ...), custom_call_target="tpu_custom_call" | custom-call | tf_op jit(solution)/shard_map/pallas_call | solution.py:553
  136.4 1.9 %copy.16 = bf16[128,2048]{1,0:T(8,128)(2,1)} copy(bf16[128,2048]{1,0:T(8,128)(2,1)} %shard_map.136) | data formatting | bytes 1048576
